TPU v7x, 32 devices: a whole 2x2x4 slice. The times are simulated.
32 devices in a mesh: ep: 4 (over y, x), tp: 8 (over z, core).
Axes of the slice: x: 2, y: 2, z: 4, core: 2. Of those that a mesh axis runs over, the one named last changes fastest.
Arguments:
- tokens: bfloat16 [128, 4096], P('ep'), may hold values from -6 to 6
- norm_gain: float32 [4096], replicated, may hold values from 0.1 to 1.9
- group_ids: int32 [128, 1], P('ep'), may hold values from 0 to 1; in each aligned block of 32 rows (0 to 31, 32 to 63, ...) at most 32 rows name the same one
- local_ids: int32 [128, 4], P('ep'), may hold values from 0 to 7, all different within a row
- group_gate: float32 [128], P('ep'), may hold values from 0.3 to 1
- expert_gate: float32 [128, 4], P('ep'), may hold values from 0.1 to 1
- lengths: int32 [32], P('ep'), may hold values from 1 to 4, 64 in all
- w_gate: bfloat16 [16, 1024, 4096], P('ep', 'tp'), may hold values from -0.09375 to 0.09375
- w_up: bfloat16 [16, 1024, 4096], P('ep', 'tp'), may hold values from -0.09375 to 0.09375
- w_down: bfloat16 [16, 1024, 4096], P('ep', None, 'tp'), may hold values from -0.1875 to 0.1875
Outputs:
- mixed: bfloat16 [128, 4096], P('ep', 'tp')
Inputs may be any that keep to these rules, and one draw needn't show every extreme that they name: `group_ids`: among the 32 rows of one index of ep no group is named by more than 32 rows, and some index reaches 32. `local_ids`: each row names 4 different experts of its group. `lengths`: the first that many of a sequence's 4 positions are live.
All inputs are finite; a program needn't handle non-finite values. No bound on the sum of `lengths` on one device may be relied on, other than what follows from the above.
Results may differ from a plain program's by a relative error of at most 0.0065.
Values may be sent and summed in bfloat16 or wider, within the bound.
A program may use at most 64 MiB of HBM per device.

v0:
```python
import jax
import jax.numpy as jnp
from jax import lax
from jax.sharding import PartitionSpec as P

EXP_PER_GROUP = 8
STEP_TOK = 4


def norm_rows(tokens, norm_gain):
    values = tokens.astype(jnp.float32)
    scale = lax.rsqrt(jnp.mean(values * values, axis=1, keepdims=True) + 1e-06)
    return (values * scale * norm_gain).astype(jnp.bfloat16)


def live_mask(lengths, tok_rows):
    places = jnp.arange(tok_rows, dtype=jnp.int32)
    within = places % STEP_TOK
    owner = places // STEP_TOK
    seq_ids = jnp.arange(lengths.shape[0], dtype=jnp.int32)
    hits = (owner[:, None] == seq_ids[None, :]) & (within[:, None] < lengths[None, :])
    return jnp.any(hits, axis=1).astype(jnp.float32)


def expert_hidden(rows, w_gate, w_up):
    gate_part = jnp.einsum("rd,efd->ref", rows, w_gate, preferred_element_type=jnp.float32)
    up_part = jnp.einsum("rd,efd->ref", rows, w_up, preferred_element_type=jnp.float32)
    return (jax.nn.silu(gate_part) * up_part).astype(jnp.bfloat16)


def local(
    tokens, norm_gain, group_ids, local_ids, group_gate, expert_gate, lengths, w_gate, w_up, w_down
):
    highest = lax.Precision.HIGHEST
    tok_rows = tokens.shape[0]
    exp_dev = w_gate.shape[0]
    width_part = w_down.shape[2]
    ep_size = lax.axis_size("ep")
    groups = exp_dev * ep_size // EXP_PER_GROUP
    normed = norm_rows(tokens, norm_gain)
    live = live_mask(lengths, tok_rows)
    local_cols = jnp.arange(EXP_PER_GROUP, dtype=jnp.int32)
    picks = (local_ids[:, :, None] == local_cols[None, None, :]).astype(jnp.float32)
    weights = expert_gate * (group_gate * live)[:, None]
    dense = jnp.sum(picks * weights[:, :, None], axis=1)
    group_cols = jnp.arange(groups, dtype=jnp.int32)
    member_int = (group_ids == group_cols[None, :]).astype(jnp.int32)
    member = member_int.astype(jnp.float32)
    capacity = 2 * tok_rows // groups
    counts = jnp.cumsum(member_int, axis=0)
    rank = jnp.sum((counts - 1) * member_int, axis=1)
    slot_ids = jnp.arange(capacity, dtype=jnp.int32)
    select = member.T[:, None, :] * (rank[None, None, :] == slot_ids[None, :, None]).astype(
        jnp.float32
    )
    rows_by_group = jnp.einsum(
        "gct,td->gcd", select.astype(jnp.bfloat16), normed, preferred_element_type=jnp.float32
    ).astype(jnp.bfloat16)
    gates_by_group = jnp.einsum("gct,tl->gcl", select, dense, precision=highest)
    share = EXP_PER_GROUP // exp_dev
    send_rows = jnp.repeat(rows_by_group, share, axis=0)
    send_gates = gates_by_group.reshape(groups, capacity, share, exp_dev).transpose(0, 2, 1, 3)
    send_gates = send_gates.reshape(ep_size, capacity, exp_dev)
    recv_rows = lax.all_to_all(send_rows, "ep", split_axis=0, concat_axis=0, tiled=True)
    recv_gates = lax.all_to_all(send_gates, "ep", split_axis=0, concat_axis=0, tiled=True)
    slot_rows = recv_rows.reshape(ep_size * capacity, recv_rows.shape[2])
    slot_gates = recv_gates.reshape(ep_size * capacity, exp_dev)
    hidden = expert_hidden(slot_rows, w_gate, w_up)
    total = jnp.einsum(
        "ref,efd->red",
        lax.all_gather(hidden, "tp", axis=2, tiled=True),
        w_down,
        preferred_element_type=jnp.float32,
    )
    results = jnp.einsum("re,red->rd", slot_gates, total, precision=highest)
    results = results.reshape(ep_size, capacity, width_part)
    back = lax.all_to_all(results, "ep", split_axis=0, concat_axis=0, tiled=True)
    grouped = jnp.sum(back.reshape(groups, share, capacity, width_part), axis=1)
    mixed = jnp.einsum("gct,gcd->td", select, grouped, precision=highest)
    return mixed.astype(jnp.bfloat16)


def solution(mesh):
    in_specs = (
        P("ep", None),
        P(),
        P("ep", None),
        P("ep", None),
        P("ep"),
        P("ep", None),
        P("ep"),
        P("ep", "tp", None),
        P("ep", "tp", None),
        P("ep", None, "tp"),
    )
    out_specs = P("ep", "tp")
    return jax.shard_map(local, mesh=mesh, in_specs=in_specs, out_specs=out_specs, check_vma=False)
```

profile of v0, /device:TPU:0, one launch (start us, length us, event | category | flops | bytes accessed | tf_op | source)
XLA Modules:
  0.0 81.1 jit_solution(2347612556403566781)
XLA Ops:
  6.5 0.7 fusion.25
  7.2 0.7 fusion.17
  7.9 1.1 %fusion.4 = f32[32]{0:T(128)S(1)} fusion(bf16[32,4096]{1,0:T(8,128)(2,1)} %param.10), kind=kLoop, calls=%fused_computation.10 | loop fusion | flops 393184 | bytes 262272 | tf_op jit(solution)/shard_map/reduce_sum | solution.py:12
  9.1 1.0 %select_reduce_fusion.1 = s32[32]{0:T(128)S(1)} fusion(s32[32,2]{1,0:T(8,128)S(1)} %reduce_window_sum.11, s32[32]{0:T(128)} %bitcast.46), kind=kLoop, calls=%fused_computation.27 | loop fusion | flops 224 | bytes 512 | tf_op jit(solution)/shard_map/reduce_sum | solution.py:51
  10.2 1.6 %convolution_convert_fusion = bf16[2,32,4096]{2,1,0:T(8,128)(2,1)S(1)} fusion(bf16[32,4096]{1,0:T(8,128)(2,1)} %param.10, f32[4096]{0:T(1024)} %param.11, f32[32]{0:T(128)S(1)} %add_rsqrt_fusion, f32[32,32]{0,1:T(8,128)S(1)} %fusion.21, f32[2,32]{1,0:T(2,128)S(1)} %fusion.25), kind=kOutput, calls=%fused_computation | convolution fusion | flops 17567744 | bytes 807296 | tf_op jit(solution)/shard_map/gct,td->gcd/dot_general | solution.py:56
  11.7 0.1 broadcast_in_dim.2
  11.8 19.4 %all_to_all.15 = bf16[4,32,4096]{2,1,0:T(8,128)(2,1)S(1)} all-to-all(bf16[4,32,4096]{2,1,0:T(8,128)(2,1)S(1)} %bitcast.37), channel_id=1, replica_groups=mesh['ep'=4,'tp'=8] {'ep'}, dimensions={0} | all-to-all | bytes 2097152 | tf_op jit(solution)/shard_map/all_to_all | solution.py:64
  31.3 1.5 %fusion.27 = f32[128,4,128]{2,0,1:T(8,128)S(1)} fusion(bf16[128,4096,1]{1,0,2:T(8,128)(2,1)S(1)} %bitcast.38, bf16[4,128,4096]{2,1,0:T(8,128)(2,1)S(1)} %copy-done), kind=kOutput, calls=%fused_computation.51 | convolution fusion | flops 536870912 | bytes 5505024 | tf_op jit(solution)/shard_map/rd,efd->ref/dot_general | solution.py:26
  32.8 2.2 %fusion = bf16[128,4,128]{2,0,1:T(8,128)(2,1)} fusion(bf16[128,4096,1]{1,0,2:T(8,128)(2,1)S(1)} %bitcast.39, bf16[4,128,4096]{2,1,0:T(8,128)(2,1)S(1)} %copy-done.4, f32[128,4,128]{2,0,1:T(8,128)S(1)} %fusion.27), kind=kOutput, calls=%fused_computation.3 | convolution fusion | flops 537264128 | bytes 5636096 | tf_op jit(solution)/shard_map/rd,efd->ref/dot_general | solution.py:27
  35.1 0.1 fusion.24
  35.2 0.2 fusion.12
  35.4 0.1 pad_maximum_fusion
  35.5 0.1 reshape.102
  35.6 0.1 reshape.115
  35.7 7.0 %all_to_all.16 = f32[4,1,128]{2,1,0:T(1,128)S(1)} all-to-all(f32[4,1,128]{2,1,0:T(1,128)S(1)} %reshape.115), channel_id=1, replica_groups=mesh['ep'=4,'tp'=8] {'ep'}, dimensions={0} | all-to-all | bytes 4096 | tf_op jit(solution)/shard_map/all_to_all | solution.py:65
  42.7 0.5 broadcast.120
  43.2 0.7 reduce
  43.9 0.1 reshape.116
  44.0 0.1 copy.43
  44.1 14.7 %all-gather.2.cloned.1.call-done = bf16[128,4,1024]{2,0,1:T(8,128)(2,1)} async-done(((bf16[128,4,128]{2,0,1:T(8,128)(2,1)}), bf16[128,4,1024]{2,0,1:T(8,128)(2,1)}) %all-gather.2.cloned.1.call-update) | async-done | bytes 1048592 | tf_op jit(solution)/shard_map/all_gather | solution.py:71
  58.8 3.2 %convolution_bitcast_fusion = f32[128,4,512]{2,0,1:T(8,128)S(1)} fusion(bf16[128,4,1024]{2,0,1:T(8,128)(2,1)} %all-gather.2.cloned.1.call-done, bf16[4,1024,512]{2,1,0:T(8,128)(2,1)} %param.19), kind=kOutput, calls=%fused_computation.1 | convolution fusion | flops 536870912 | bytes 6291456 | tf_op jit(solution)/shard_map/ref,efd->red/dot_general | solution.py:69
  62.0 2.4 %fusion.2 = f32[128,1,512]{2,1,0:T(1,128)S(1)} fusion(f32[128,4,1]{1,2,0:T(1,128)S(1)} %bitcast.41, f32[128,4,512]{2,0,1:T(8,128)S(1)} %convolution_bitcast_fusion), kind=kOutput, calls=%fused_computation.6 | convolution fusion | flops 3145728 | bytes 1312768 | tf_op jit(solution)/shard_map/re,red->rd/dot_general | solution.py:75
  64.5 8.8 %all_to_all.17 = f32[4,32,512]{2,1,0:T(8,128)S(1)} all-to-all(f32[4,32,512]{2,1,0:T(8,128)S(1)} %bitcast.40), channel_id=1, replica_groups=mesh['ep'=4,'tp'=8] {'ep'}, dimensions={0} | all-to-all | bytes 524288 | tf_op jit(solution)/shard_map/all_to_all | solution.py:77
  73.3 0.9 %fusion.1 = bf16[32,512]{1,0:T(8,128)(2,1)} fusion(f32[2,32,512]{2,1,0:T(8,128)S(1)} %bitcast_reduce_fusion, f32[32,32]{0,1:T(8,128)S(1)} %fusion.21, f32[2,32]{1,0:T(2,128)S(1)} %fusion.25), kind=kOutput, calls=%fused_computation.5 | convolution fusion | flops 12601344 | bytes 168192 | tf_op jit(solution)/shard_map/gct,gcd->td/dot_general | solution.py:79
  (26 shorter events, 0.3 us)
Async XLA Ops:
  6.5 52.3 %all-gather.2.cloned.1.call-start = ((), (), s32[]{:S(2)}) async-start(), calls=%async_computation.3 | async-start | bytes 1179648 | tf_op jit(solution)/shard_map/all_gather | solution.py:71
  9.1 22.2 %copy-start = (bf16[4,128,4096]{2,1,0:T(8,128)(2,1)S(1)}, bf16[4,128,4096]{2,1,0:T(8,128)(2,1)}, u32[]{:S(2)}) copy-start(bf16[4,128,4096]{2,1,0:T(8,128)(2,1)} %param.17) | copy-start | bytes 12582916
  11.8 21.0 %copy-start.4 = (bf16[4,128,4096]{2,1,0:T(8,128)(2,1)S(1)}, bf16[4,128,4096]{2,1,0:T(8,128)(2,1)}, u32[]{:S(2)}) copy-start(bf16[4,128,4096]{2,1,0:T(8,128)(2,1)} %param.18) | copy-start | bytes 12582916
  32.8 2.3 %copy-start.3 = (s32[8]{0:T(128)S(1)}, s32[8]{0:T(128)}, u32[]{:S(2)}) copy-start(s32[8]{0:T(128)} %param.16) | copy-start | bytes 100
  32.8 2.4 %copy-start.5 = (f32[32]{0:T(128)S(1)}, f32[32]{0:T(128)}, u32[]{:S(2)}) copy-start(f32[32]{0:T(128)} %param.14) | copy-start | bytes 388
  32.8 2.4 %copy-start.1 = (f32[32,4]{0,1:T(4,128)S(1)}, f32[32,4]{0,1:T(4,128)}, u32[]{:S(2)}) copy-start(f32[32,4]{0,1:T(4,128)} %param.15) | copy-start | bytes 1540
  32.8 2.4 %copy-start.2 = (s32[32,4]{0,1:T(4,128)S(1)}, s32[32,4]{0,1:T(4,128)}, u32[]{:S(2)}) copy-start(s32[32,4]{0,1:T(4,128)} %param.13) | copy-start | bytes 1540
Sparse Core Ops, SparseCore 0:
  35.2 23.5 all-gather.1
where the time goes:
time: 81.4 us; the launch traced here: 81.1 us
  blocking collectives  35.2 us (43%)
  waiting for transfers between devices  14.7 us (18%)
  between operations  13.6 us (17%)
  matrix products  12.1 us (15%)
  other arithmetic  4.48 us (6%)
  local copies, waits for them, and re-layouts  1.06 us (1%)
    all_to_all x1, blocking collectives, local(): lax.all_to_all(send_rows, 'ep', split_axis=0, concat_axis=0, tiled=True)  19.4 us
    all_gather x1, waiting for transfers between devices, local(): lax.all_gather(hidden, 'tp', axis=2, tiled=True)  14.7 us
    all_to_all x1, blocking collectives, local(): lax.all_to_all(results, 'ep', split_axis=0, concat_axis=0, tiled=True)  8.79 us
    all_to_all x1, blocking collectives, local(): lax.all_to_all(send_gates, 'ep', split_axis=0, concat_axis=0, tiled=True)  7.01 us
    dot_general x1, matrix products, local(): jnp.einsum('ref,efd->red', lax.all_gather(hidden, 'tp', axis=2, tiled=Tru...  3.23 us
    dot_general x1, matrix products, local(): results = jnp.einsum('re,red->rd', slot_gates, total, precision=highest)  2.43 us
    dot_general x1, matrix products, expert_hidden(): jnp.einsum('rd,efd->ref', rows, w_up, preferred_element_type=jnp.float32)  2.18 us
  transfers between devices with their start and end apart: 1, of which 1 were waited for; matrix products, arithmetic and copies ran while one was open for 2% of the time, Pallas kernels for 0%

commit v1 on v0

--- a/solution.py
+++ b/solution.py
@@ -5,6 +5,18 @@
 
 EXP_PER_GROUP = 8
 STEP_TOK = 4
+
+
+def ring_product(x, axis, dim, term):
+    length, index, extent = (lax.axis_size(axis), lax.axis_index(axis), x.shape[dim])
+    forward = [(i, (i + 1) % length) for i in range(length)]
+    current, total = (x, None)
+    for step in range(length):
+        upcoming = lax.ppermute(current, axis, forward) if step < length - 1 else None
+        update = term(current, (index - step) % length * extent)
+        total = update if total is None else total + update
+        current = upcoming
+    return total
 
 
 def norm_rows(tokens, norm_gain):
@@ -66,11 +78,16 @@
     slot_rows = recv_rows.reshape(ep_size * capacity, recv_rows.shape[2])
     slot_gates = recv_gates.reshape(ep_size * capacity, exp_dev)
     hidden = expert_hidden(slot_rows, w_gate, w_up)
-    total = jnp.einsum(
-        "ref,efd->red",
-        lax.all_gather(hidden, "tp", axis=2, tiled=True),
-        w_down,
-        preferred_element_type=jnp.float32,
+    total = ring_product(
+        hidden,
+        "tp",
+        2,
+        lambda own_block, offset: jnp.einsum(
+            "ref,efd->red",
+            own_block,
+            lax.dynamic_slice_in_dim(w_down, offset, own_block.shape[2], axis=1),
+            preferred_element_type=jnp.float32,
+        ),
     )
     results = jnp.einsum("re,red->rd", slot_gates, total, precision=highest)
     results = results.reshape(ep_size, capacity, width_part)

time: 81.4 us -> 92.1 us (1.13)
  waiting for transfers between devices: 14.7 us -> 53.3 us
  blocking collectives: 35.2 us -> 8.26 us
  between operations: 13.6 us -> 0.32 us
  starting transfers between devices: 0.01 us -> 8.78 us
  other arithmetic: 4.48 us -> 7 us
  local copies, waits for them, and re-layouts: 1.06 us -> 3.28 us
  matrix products: 12.1 us -> 10.7 us
    ppermute x0 -> x7, waiting for transfers between devices: none -> 40.2 us  [ring_product(): lax.ppermute(current, axis, forward)]
    all_to_all x2 -> x0, blocking collectives: 26.4 us -> none  [the longest x1 19.4 us: local(): lax.all_to_all(send_rows, 'ep', split_axis=0, concat_axis=0, tiled=True)]
    all_gather x1 -> x0, waiting for transfers between devices: 14.7 us -> none  [local(): lax.all_gather(hidden, 'tp', axis=2, tiled=True)]
    all_to_all x0 -> x2, waiting for transfers between devices: none -> 13.1 us  [the longest x1 10.9 us: local(): lax.all_to_all(send_rows, 'ep', split_axis=0, concat_axis=0, tiled=True)]
    all_to_all x0 -> x2, starting transfers between devices: none -> 8.71 us  [the longest x1 5.19 us: local(): lax.all_to_all(send_gates, 'ep', split_axis=0, concat_axis=0, tiled=True)]
    dot_general x2 -> x8, matrix products: 5.65 us -> 2.83 us  [local(): jnp.einsum('ref,efd->red', own_block, lax.dynamic_slice_in_dim(w_down, of...]
    dot_general x1, matrix products: 1.53 us -> 3.86 us  [expert_hidden(): jnp.einsum('rd,efd->ref', rows, w_gate, preferred_element_type=jnp.float32)]
    mul x2, other arithmetic: 0.01 us -> 1.34 us  [local(): weights = expert_gate * (group_gate * live)[:, None]]
  transfers between devices with their start and end apart: 1 -> 9, of which waited for: 1 -> 9; matrix products, arithmetic and copies ran while one was open for 2% -> 7% of each run, Pallas kernels for 0% -> 0%
where the time goes in v1:
time: 92.1 us; the launch traced here: 91.6 us
  waiting for transfers between devices  53.3 us (58%)
  matrix products  10.7 us (12%)
  starting transfers between devices  8.78 us (10%)
  blocking collectives  8.26 us (9%)
  other arithmetic  7 us (8%)
  local copies, waits for them, and re-layouts  3.28 us (4%)
    ppermute x7, waiting for transfers between devices, ring_product(): lax.ppermute(current, axis, forward)  40.2 us
    all_to_all x1, waiting for transfers between devices, local(): lax.all_to_all(send_rows, 'ep', split_axis=0, concat_axis=0, tiled=True)  10.9 us
    all_to_all x1, blocking collectives, local(): lax.all_to_all(results, 'ep', split_axis=0, concat_axis=0, tiled=True)  8.26 us
    all_to_all x1, starting transfers between devices, local(): lax.all_to_all(send_gates, 'ep', split_axis=0, concat_axis=0, tiled=True)  5.19 us
    dot_general x1, matrix products, expert_hidden(): jnp.einsum('rd,efd->ref', rows, w_gate, preferred_element_type=jnp.float32)  3.86 us
    all_to_all x1, starting transfers between devices, local(): lax.all_to_all(send_rows, 'ep', split_axis=0, concat_axis=0, tiled=True)  3.51 us
    dot_general x8, matrix products, local(): jnp.einsum('ref,efd->red', own_block, lax.dynamic_slice_in_dim(w_down, of...  2.83 us
    all_to_all x1, waiting for transfers between devices, local(): lax.all_to_all(send_gates, 'ep', split_axis=0, concat_axis=0, tiled=True)  2.12 us
  transfers between devices with their start and end apart: 9, of which 9 were waited for; matrix products, arithmetic and copies ran while one was open for 7% of the time, Pallas kernels for 0%

profile of v1, /device:TPU:0, one launch (start us, length us, event | category | flops | bytes accessed | tf_op | source)
XLA Modules:
  0.0 91.6 jit_solution(948554881292509612)
XLA Ops:
  0.0 0.7 fusion.27
  1.4 0.8 select_reduce_fusion.1
  2.4 0.7 fusion.34
  3.8 0.7 broadcast_multiply_fusion
  4.4 0.7 select_reduce_fusion
  5.5 0.7 reshape.114
  6.2 5.2 %all-to-all-start = ((f32[4,1,128]{2,1,0:T(1,128)}), f32[4,1,128]{2,1,0:T(1,128)S(1)}, u32[]{:S(2)}, u32[]{:S(2)}) async-start(f32[4,1,128]{2,1,0:T(1,128)} %reshape.114), calls=%async_computation | async-start | bytes 4096 | tf_op jit(solution)/shard_map/all_to_all | solution.py:77
  11.4 1.1 %fusion.5 = f32[32]{0:T(128)S(1)} fusion(bf16[32,4096]{1,0:T(8,128)(2,1)} %param.10), kind=kLoop, calls=%fused_computation.17 | loop fusion | flops 393184 | bytes 262272 | tf_op jit(solution)/shard_map/reduce_sum | solution.py:24
  12.5 1.4 %convolution_convert_fusion = bf16[2,32,4096]{2,1,0:T(8,128)(2,1)S(1)} fusion(bf16[32,4096]{1,0:T(8,128)(2,1)} %param.10, f32[4096]{0:T(1024)} %param.11, f32[32]{0:T(128)S(1)} %add_rsqrt_fusion, f32[32,32]{0,1:T(8,128)S(1)} %fusion.31, f32[2,32]{1,0:T(2,128)S(1)} %fusion.43), kind=kOutput, calls=%fused_computation | convolution fusion | flops 17567744 | bytes 807296 | tf_op jit(solution)/shard_map/gct,td->gcd/dot_general | solution.py:68
  13.9 2.1 %all-to-all-done = f32[4,1,128]{2,1,0:T(1,128)S(1)} async-done(((f32[4,1,128]{2,1,0:T(1,128)}), f32[4,1,128]{2,1,0:T(1,128)S(1)}, u32[]{:S(2)}, u32[]{:S(2)}) %all-to-all-start) | async-done | bytes 2080 | tf_op jit(solution)/shard_map/all_to_all | solution.py:77
  16.0 1.1 %broadcast_in_dim.2 = bf16[2,2,32,4096]{3,2,1,0:T(8,128)(2,1)} broadcast(bf16[2,32,4096]{2,1,0:T(8,128)(2,1)S(1)} %convolution_convert_fusion), dimensions={0,2,3} | broadcast | bytes 1572864 | tf_op jit(solution)/shard_map/broadcast_in_dim | solution.py:73
  17.1 3.5 %all-to-all-start.1 = ((bf16[4,32,4096]{2,1,0:T(8,128)(2,1)}), bf16[4,32,4096]{2,1,0:T(8,128)(2,1)S(1)}, u32[]{:S(2)}, u32[]{:S(2)}) async-start(bf16[4,32,4096]{2,1,0:T(8,128)(2,1)} %bitcast.3), calls=%async_computation.1 | async-start | bytes 2097152 | tf_op jit(solution)/shard_map/all_to_all | solution.py:76
  22.1 10.9 %all-to-all-done.1 = bf16[4,32,4096]{2,1,0:T(8,128)(2,1)S(1)} async-done(((bf16[4,32,4096]{2,1,0:T(8,128)(2,1)}), bf16[4,32,4096]{2,1,0:T(8,128)(2,1)S(1)}, u32[]{:S(2)}, u32[]{:S(2)}) %all-to-all-start.1) | async-done | bytes 1048608 | tf_op jit(solution)/shard_map/all_to_all | solution.py:76
  33.1 3.9 %fusion.45 = f32[128,4,128]{2,0,1:T(8,128)S(1)} fusion(bf16[128,4096,1]{1,0,2:T(8,128)(2,1)S(1)} %bitcast.45, bf16[4,128,4096]{2,1,0:T(8,128)(2,1)} %param.17), kind=kOutput, calls=%fused_computation.75 | convolution fusion | flops 536870912 | bytes 5505024 | tf_op jit(solution)/shard_map/rd,efd->ref/dot_general | solution.py:38
  37.0 1.5 %fusion.3 = bf16[128,4,128]{2,0,1:T(8,128)(2,1)S(1)} fusion(bf16[128,4096,1]{1,0,2:T(8,128)(2,1)S(1)} %bitcast.46, bf16[4,128,4096]{2,1,0:T(8,128)(2,1)S(1)} %copy-done.1, f32[128,4,128]{2,0,1:T(8,128)S(1)} %fusion.45), kind=kOutput, calls=%fused_computation.12 | convolution fusion | flops 537264128 | bytes 5636096 | tf_op jit(solution)/shard_map/rd,efd->ref/dot_general | solution.py:39
  39.5 5.2 %collective-permute-done = bf16[128,4,128]{2,0,1:T(8,128)(2,1)S(1)} collective-permute-done((bf16[128,4,128]{2,0,1:T(8,128)(2,1)S(1)}, bf16[128,4,128]{2,0,1:T(8,128)(2,1)S(1)}, u32[]{:S(2)}, u32[]{:S(2)}) %collective-permute-start) | collective-permute-done | bytes 131104 | tf_op jit(solution)/shard_map/ppermute | solution.py:15
  45.1 5.8 %collective-permute-done.1 = bf16[128,4,128]{2,0,1:T(8,128)(2,1)S(1)} collective-permute-done((bf16[128,4,128]{2,0,1:T(8,128)(2,1)S(1)}, bf16[128,4,128]{2,0,1:T(8,128)(2,1)S(1)}, u32[]{:S(2)}, u32[]{:S(2)}) %collective-permute-start.1) | collective-permute-done | bytes 131104 | tf_op jit(solution)/shard_map/ppermute | solution.py:15
  51.3 5.8 %collective-permute-done.2 = bf16[128,4,128]{2,0,1:T(8,128)(2,1)S(1)} collective-permute-done((bf16[128,4,128]{2,0,1:T(8,128)(2,1)S(1)}, bf16[128,4,128]{2,0,1:T(8,128)(2,1)S(1)}, u32[]{:S(2)}, u32[]{:S(2)}) %collective-permute-start.2) | collective-permute-done | bytes 131104 | tf_op jit(solution)/shard_map/ppermute | solution.py:15
  57.5 5.8 %collective-permute-done.3 = bf16[128,4,128]{2,0,1:T(8,128)(2,1)S(1)} collective-permute-done((bf16[128,4,128]{2,0,1:T(8,128)(2,1)S(1)}, bf16[128,4,128]{2,0,1:T(8,128)(2,1)S(1)}, u32[]{:S(2)}, u32[]{:S(2)}) %collective-permute-start.3) | collective-permute-done | bytes 131104 | tf_op jit(solution)/shard_map/ppermute | solution.py:15
  63.7 5.8 %collective-permute-done.4 = bf16[128,4,128]{2,0,1:T(8,128)(2,1)S(1)} collective-permute-done((bf16[128,4,128]{2,0,1:T(8,128)(2,1)S(1)}, bf16[128,4,128]{2,0,1:T(8,128)(2,1)S(1)}, u32[]{:S(2)}, u32[]{:S(2)}) %collective-permute-start.4) | collective-permute-done | bytes 131104 | tf_op jit(solution)/shard_map/ppermute | solution.py:15
  69.9 5.8 %collective-permute-done.5 = bf16[128,4,128]{2,0,1:T(8,128)(2,1)S(1)} collective-permute-done((bf16[128,4,128]{2,0,1:T(8,128)(2,1)S(1)}, bf16[128,4,128]{2,0,1:T(8,128)(2,1)S(1)}, u32[]{:S(2)}, u32[]{:S(2)}) %collective-permute-start.5) | collective-permute-done | bytes 131104 | tf_op jit(solution)/shard_map/ppermute | solution.py:15
  76.1 5.8 %collective-permute-done.6 = bf16[128,4,128]{2,0,1:T(8,128)(2,1)S(1)} collective-permute-done((bf16[128,4,128]{2,0,1:T(8,128)(2,1)S(1)}, bf16[128,4,128]{2,0,1:T(8,128)(2,1)S(1)}, u32[]{:S(2)}, u32[]{:S(2)}) %collective-permute-start.6) | collective-permute-done | bytes 131104 | tf_op jit(solution)/shard_map/ppermute | solution.py:15
  82.4 8.3 %all_to_all.15 = f32[4,32,512]{2,1,0:T(8,128)S(1)} all-to-all(f32[4,32,512]{2,1,0:T(8,128)S(1)} %bitcast.47), channel_id=1, replica_groups=mesh['ep'=4,'tp'=8] {'ep'}, dimensions={0} | all-to-all | bytes 524288 | tf_op jit(solution)/shard_map/all_to_all | solution.py:94
  90.7 0.9 %fusion.4 = bf16[32,512]{1,0:T(8,128)(2,1)} fusion(f32[2,32,512]{2,1,0:T(8,128)S(1)} %bitcast_reduce_fusion, f32[32,32]{0,1:T(8,128)S(1)} %fusion.31, f32[2,32]{1,0:T(2,128)S(1)} %fusion.43), kind=kOutput, calls=%fused_computation.14 | convolution fusion | flops 12601344 | bytes 168192 | tf_op jit(solution)/shard_map/gct,gcd->td/dot_general | solution.py:96
  (38 shorter events, 6.8 us)
Async XLA Ops:
  6.2 9.8 %all-to-all-start = ((f32[4,1,128]{2,1,0:T(1,128)}), f32[4,1,128]{2,1,0:T(1,128)S(1)}, u32[]{:S(2)}, u32[]{:S(2)}) async-start(f32[4,1,128]{2,1,0:T(1,128)} %reshape.114), calls=%async_computation | async-start | bytes 4096 | tf_op jit(solution)/shard_map/all_to_all | solution.py:77
  17.1 16.0 %all-to-all-start.1 = ((bf16[4,32,4096]{2,1,0:T(8,128)(2,1)}), bf16[4,32,4096]{2,1,0:T(8,128)(2,1)S(1)}, u32[]{:S(2)}, u32[]{:S(2)}) async-start(bf16[4,32,4096]{2,1,0:T(8,128)(2,1)} %bitcast.3), calls=%async_computation.1 | async-start | bytes 2097152 | tf_op jit(solution)/shard_map/all_to_all | solution.py:76
  33.1 3.9 %copy-start.1 = (bf16[4,128,4096]{2,1,0:T(8,128)(2,1)S(1)}, bf16[4,128,4096]{2,1,0:T(8,128)(2,1)}, u32[]{:S(2)}) copy-start(bf16[4,128,4096]{2,1,0:T(8,128)(2,1)} %param.18) | copy-start | bytes 12582916
  36.9 2.2 %copy-start = (bf16[4,1024,512]{2,1,0:T(8,128)(2,1)S(1)}, bf16[4,1024,512]{2,1,0:T(8,128)(2,1)}, u32[]{:S(2)}) copy-start(bf16[4,1024,512]{2,1,0:T(8,128)(2,1)} %param.19) | copy-start | bytes 12582916
  38.5 6.2 %collective-permute-start = (bf16[128,4,128]{2,0,1:T(8,128)(2,1)S(1)}, bf16[128,4,128]{2,0,1:T(8,128)(2,1)S(1)}, u32[]{:S(2)}, u32[]{:S(2)}) collective-permute-start(bf16[128,4,128]{2,0,1:T(8,128)(2,1)S(1)} %fusion.3), channel_id=1, source_target_pairs={{0,1},{1,2},{2,3},{3,4},{4,5},{5,6},{6,7},{7,0},{8,9},{9,10},{10,1... | collective-permute-start | bytes 393224 | tf_op jit(solution)/shard_map/ppermute | solution.py:15
  44.7 6.2 %collective-permute-start.1 = (bf16[128,4,128]{2,0,1:T(8,128)(2,1)S(1)}, bf16[128,4,128]{2,0,1:T(8,128)(2,1)S(1)}, u32[]{:S(2)}, u32[]{:S(2)}) collective-permute-start(bf16[128,4,128]{2,0,1:T(8,128)(2,1)S(1)} %collective-permute-done), channel_id=1, source_target_pairs={{0,1},{1,2},{2,3},{3,4},{4,5},{5,6},{6,7},{7,0},{8,9},{9,10},{10,1... | collective-permute-start | bytes 393224 | tf_op jit(solution)/shard_map/ppermute | solution.py:15
  50.9 6.2 %collective-permute-start.2 = (bf16[128,4,128]{2,0,1:T(8,128)(2,1)S(1)}, bf16[128,4,128]{2,0,1:T(8,128)(2,1)S(1)}, u32[]{:S(2)}, u32[]{:S(2)}) collective-permute-start(bf16[128,4,128]{2,0,1:T(8,128)(2,1)S(1)} %collective-permute-done.1), channel_id=1, source_target_pairs={{0,1},{1,2},{2,3},{3,4},{4,5},{5,6},{6,7},{7,0},{8,9},{9,10},{10,1... | collective-permute-start | bytes 393224 | tf_op jit(solution)/shard_map/ppermute | solution.py:15
  57.1 6.2 %collective-permute-start.3 = (bf16[128,4,128]{2,0,1:T(8,128)(2,1)S(1)}, bf16[128,4,128]{2,0,1:T(8,128)(2,1)S(1)}, u32[]{:S(2)}, u32[]{:S(2)}) collective-permute-start(bf16[128,4,128]{2,0,1:T(8,128)(2,1)S(1)} %collective-permute-done.2), channel_id=1, source_target_pairs={{0,1},{1,2},{2,3},{3,4},{4,5},{5,6},{6,7},{7,0},{8,9},{9,10},{10,1... | collective-permute-start | bytes 393224 | tf_op jit(solution)/shard_map/ppermute | solution.py:15
  63.3 6.2 %collective-permute-start.4 = (bf16[128,4,128]{2,0,1:T(8,128)(2,1)S(1)}, bf16[128,4,128]{2,0,1:T(8,128)(2,1)S(1)}, u32[]{:S(2)}, u32[]{:S(2)}) collective-permute-start(bf16[128,4,128]{2,0,1:T(8,128)(2,1)S(1)} %collective-permute-done.3), channel_id=1, source_target_pairs={{0,1},{1,2},{2,3},{3,4},{4,5},{5,6},{6,7},{7,0},{8,9},{9,10},{10,1... | collective-permute-start | bytes 393224 | tf_op jit(solution)/shard_map/ppermute | solution.py:15
  69.5 6.2 %collective-permute-start.5 = (bf16[128,4,128]{2,0,1:T(8,128)(2,1)S(1)}, bf16[128,4,128]{2,0,1:T(8,128)(2,1)S(1)}, u32[]{:S(2)}, u32[]{:S(2)}) collective-permute-start(bf16[128,4,128]{2,0,1:T(8,128)(2,1)S(1)} %collective-permute-done.4), channel_id=1, source_target_pairs={{0,1},{1,2},{2,3},{3,4},{4,5},{5,6},{6,7},{7,0},{8,9},{9,10},{10,1... | collective-permute-start | bytes 393224 | tf_op jit(solution)/shard_map/ppermute | solution.py:15
  75.7 6.2 %collective-permute-start.6 = (bf16[128,4,128]{2,0,1:T(8,128)(2,1)S(1)}, bf16[128,4,128]{2,0,1:T(8,128)(2,1)S(1)}, u32[]{:S(2)}, u32[]{:S(2)}) collective-permute-start(bf16[128,4,128]{2,0,1:T(8,128)(2,1)S(1)} %collective-permute-done.5), channel_id=1, source_target_pairs={{0,1},{1,2},{2,3},{3,4},{4,5},{5,6},{6,7},{7,0},{8,9},{9,10},{10,1... | collective-permute-start | bytes 393224 | tf_op jit(solution)/shard_map/ppermute | solution.py:15
